TPU v7x, 32 devices: a whole 2x2x4 slice. The times are simulated.
32 devices in a mesh: sp: 16 (over z, y, x), tp: 2 (over core).
Axes of the slice: x: 2, y: 2, z: 4, core: 2. Of those that a mesh axis runs over, the one named last changes fastest.
Arguments:
- residual: bfloat16 [2048, 2048], P('sp'), may hold values from -6 to 6
- query_nope: bfloat16 [2048, 8, 128], P('sp', 'tp'), may hold values from -6 to 6
- query_rope: bfloat16 [2048, 8, 64], P('sp', 'tp'), may hold values from -64 to 64
- latent: bfloat16 [2048, 256], P('sp'), may hold values from -6 to 6
- rope_key: bfloat16 [2048, 64], P('sp'), may hold values from -64 to 64
- kv_gain: bfloat16 [256], replicated, may hold values from 0.099609375 to 1.8984375
- key_up: bfloat16 [256, 8, 128], replicated, may hold values from -0.375 to 0.375
- value_up: bfloat16 [256, 8, 128], replicated, may hold values from -0.375 to 0.375
- out_weight: bfloat16 [1024, 2048], P('tp'), may hold values from -0.1875 to 0.1875
- post_gain: bfloat16 [2048], replicated, may hold values from 0.099609375 to 1.8984375
- pre_gain: bfloat16 [2048], replicated, may hold values from 0.099609375 to 1.8984375
- ffn_gain: bfloat16 [2048], replicated, may hold values from 0.099609375 to 1.8984375
- up_value: bfloat16 [2048, 5632], P('sp', 'tp'), may hold values from -0.125 to 0.125
- up_gate: bfloat16 [2048, 5632], P('sp', 'tp'), may hold values from -0.125 to 0.125
- conv_value: bfloat16 [3, 5632], replicated, may hold values from -3.5 to 3.5
- conv_gate: bfloat16 [3, 5632], replicated, may hold values from -3.5 to 3.5
- down_weight: bfloat16 [5632, 2048], P('tp', 'sp'), may hold values from -0.078125 to 0.078125
Outputs:
- layer_out: bfloat16 [2048, 2048], P(('sp', 'tp'))
All inputs are finite; a program needn't handle non-finite values.
Results may differ from a plain program's by a relative error of at most 0.02.
Values may be sent and summed in bfloat16 or wider, within the bound.
No kernel may reach another device: no remote copies, remote signals or barrier semaphores. Data moves between devices by JAX's collectives and lax.ppermute only.
A program may use at most 128 MiB of HBM per device.

v0:
```python
import jax
import jax.numpy as jnp
from jax import lax
from jax.sharding import PartitionSpec as P

GRID = 64
epsilon = 1e-06
rope_base = 10000.0


def extended(x, sides, width):
    for axis, dim in sides:
        size, length = (lax.axis_size(axis), x.shape[dim])
        up = [(i, (i + 1) % size) for i in range(size - 1)]
        down = [(j, i) for i, j in up]
        last = lax.slice_in_dim(x, length - width, length, axis=dim)
        initial = lax.slice_in_dim(x, 0, width, axis=dim)
        before = lax.ppermute(last, axis, up)
        after = lax.ppermute(initial, axis, down)
        x = jnp.concatenate([before, x, after], axis=dim)
    return x


def rms_norm(values, gain):
    return (
        values
        * lax.rsqrt(jnp.mean(values * values, axis=-1, keepdims=True) + epsilon)
        * gain.astype(jnp.float32)
    )


def widened(values):
    return lax.optimization_barrier(values.astype(jnp.bfloat16)).astype(jnp.float32)


def rotate(values, positions):
    pair_count = values.shape[-1] // 4
    frequency = rope_base ** (-jnp.arange(pair_count, dtype=jnp.float32) / pair_count)
    grid_rows = (positions // GRID).astype(jnp.float32)
    grid_cols = (positions % GRID).astype(jnp.float32)
    angles = jnp.stack([grid_rows, grid_cols], axis=-1)[:, :, None] * frequency
    table_shape = (angles.shape[0],) + (1,) * (values.ndim - 2) + angles.shape[1:]
    cosine = jnp.cos(angles).reshape(table_shape)
    sine = jnp.sin(angles).reshape(table_shape)
    halves = values.reshape(values.shape[:-1] + (2, 2, pair_count))
    leading = halves[..., 0, :]
    trailing = halves[..., 1, :]
    turned = jnp.stack(
        [leading * cosine - trailing * sine, trailing * cosine + leading * sine], axis=-2
    )
    return turned.reshape(values.shape)


def body(
    residual,
    query_nope,
    query_rope,
    latent,
    rope_key,
    kv_gain,
    key_up,
    value_up,
    out_weight,
    post_gain,
    pre_gain,
    ffn_gain,
    up_value,
    up_gate,
    conv_value,
    conv_gate,
    down_weight,
):
    tok_rows = residual.shape[0]
    heads_dev = query_nope.shape[1]
    value_width = value_up.shape[2]
    tp_index = lax.axis_index("tp")
    positions = lax.axis_index("sp") * tok_rows + jnp.arange(tok_rows, dtype=jnp.int32)
    score_scale = (query_nope.shape[2] + query_rope.shape[2]) ** (-0.5)
    normed = rms_norm(latent.astype(jnp.float32), kv_gain).astype(jnp.bfloat16)
    key_turn = rotate(rope_key.astype(jnp.float32), positions).astype(jnp.bfloat16)
    query_turn = rotate(query_rope.astype(jnp.float32), positions).astype(jnp.bfloat16)
    key_local = lax.dynamic_slice_in_dim(key_up, tp_index * heads_dev, heads_dev, 1)
    value_local = lax.dynamic_slice_in_dim(value_up, tp_index * heads_dev, heads_dev, 1)
    pieces = (
        lax.all_gather(normed, "sp", axis=0, tiled=True),
        lax.all_gather(key_turn, "sp", axis=0, tiled=True),
    )
    keys_nope = jnp.einsum(
        "nc,chd->nhd", pieces[0], key_local, preferred_element_type=jnp.float32
    ).astype(jnp.bfloat16)
    values_part = jnp.einsum(
        "nc,chd->nhd", pieces[0], value_local, preferred_element_type=jnp.float32
    ).astype(jnp.bfloat16)
    row_max = jnp.full((heads_dev, tok_rows), -1e30, jnp.float32)
    scores = (
        jnp.einsum("qhd,khd->hqk", query_nope, keys_nope, preferred_element_type=jnp.float32)
        + jnp.einsum("qhd,kd->hqk", query_turn, pieces[1], preferred_element_type=jnp.float32)
    ) * score_scale
    new_max = jnp.maximum(row_max, jnp.max(scores, axis=-1))
    weights = jnp.exp(scores - new_max[:, :, None])
    totals = jnp.sum(weights, axis=-1)
    weighted = jnp.einsum(
        "hqk,khd->hqd",
        weights.astype(jnp.bfloat16),
        values_part,
        preferred_element_type=jnp.float32,
    )
    attended = (weighted / totals[:, :, None]).astype(jnp.bfloat16)
    attended = jnp.transpose(attended, (1, 0, 2)).reshape(tok_rows, heads_dev * value_width)
    row_share = tok_rows // lax.axis_size("tp")
    summed = lax.psum_scatter(
        jnp.dot(attended, out_weight, preferred_element_type=jnp.float32).astype(jnp.bfloat16),
        "tp",
        scatter_dimension=0,
        tiled=True,
    ).astype(jnp.float32)
    own_rows = lax.dynamic_slice_in_dim(residual, tp_index * row_share, row_share, 0).astype(
        jnp.float32
    )
    stream_wide = widened(own_rows + rms_norm(widened(summed), post_gain))
    inputs = lax.all_gather(
        rms_norm(stream_wide, pre_gain).astype(jnp.bfloat16), "tp", axis=0, tiled=True
    )
    ff_dev = up_value.shape[1]
    up_joined = jnp.concatenate([up_value, up_gate], axis=1)
    up_whole = lax.all_gather(up_joined, "sp", axis=0, tiled=True)
    up_pair = jnp.dot(inputs, up_whole, preferred_element_type=jnp.float32).astype(jnp.bfloat16)
    padded = extended(up_pair, (("sp", 0),), 1).astype(jnp.float32)
    channel_start = tp_index * ff_dev
    conv_taps = jnp.concatenate(
        [
            lax.dynamic_slice_in_dim(conv_value, channel_start, ff_dev, 1),
            lax.dynamic_slice_in_dim(conv_gate, channel_start, ff_dev, 1),
        ],
        axis=1,
    ).astype(jnp.float32)
    mixed_conv = (
        padded[:-2] * conv_taps[0] + padded[1:-1] * conv_taps[1] + padded[2:] * conv_taps[2]
    )
    hidden = (jax.nn.silu(mixed_conv[:, ff_dev:]) * mixed_conv[:, :ff_dev]).astype(jnp.bfloat16)
    down_whole = lax.all_gather(down_weight, "sp", axis=1, tiled=True)
    down_terms = jnp.dot(hidden, down_whole, preferred_element_type=jnp.float32)
    reduced = lax.psum_scatter(
        down_terms.astype(jnp.bfloat16), "tp", scatter_dimension=0, tiled=True
    ).astype(jnp.float32)
    return (stream_wide + rms_norm(widened(reduced), ffn_gain)).astype(jnp.bfloat16)


def solution(mesh):
    placed = (
        P("sp", None),
        P("sp", "tp", None),
        P("sp", "tp", None),
        P("sp", None),
        P("sp", None),
        P(),
        P(),
        P(),
        P("tp", None),
        P(),
        P(),
        P(),
        P("sp", "tp"),
        P("sp", "tp"),
        P(),
        P(),
        P("tp", "sp"),
    )
    return jax.shard_map(
        body, mesh=mesh, in_specs=placed, out_specs=P(("sp", "tp"), None), check_vma=False
    )
```

profile of v0, /device:TPU:0, one launch (start us, length us, event | category | flops | bytes accessed | tf_op | source)
XLA Modules:
  0.0 553.0 jit_solution(2200279591683789855)
XLA Ops:
  6.5 1.1 fusion.40
  7.6 0.7 convert_element_type.108
  8.3 1.6 fusion.42
  9.9 0.9 convert.19
  10.8 0.7 convert.18
  11.9 44.1 %all_gather.16 = bf16[2048,64]{0,1:T(8,128)(2,1)S(1)} all-gather(bf16[128,64]{0,1:T(8,128)(2,1)S(1)} %bitcast.41), channel_id=1, replica_groups=mesh['sp'=16,'tp'=2] {'sp'}, dimensions={0}, use_global_device_ids=true | all-gather | bytes 278528 | tf_op jit(solution)/shard_map/all_gather | solution.py:86
  56.0 1.5 constant_dynamic-slice_fusion.2
  57.5 10.8 %all-gather.4.cloned.1.call-done = bf16[2048,256]{1,0:T(8,128)(2,1)} async-done(((bf16[128,256]{1,0:T(8,128)(2,1)}), bf16[2048,256]{1,0:T(8,128)(2,1)}) %all-gather.4.cloned.1.call-update) | async-done | bytes 1048592 | tf_op jit(solution)/shard_map/all_gather | solution.py:85
  68.3 4.4 fusion.8
  72.7 2.9 fusion.58
  75.7 1.9 copy-done.1
  77.6 0.6 fusion.1
  78.2 4.3 fusion.16
  82.5 2.3 convolution_convert_fusion.4
  84.8 1.2 pad_maximum_fusion
  86.1 0.5 all-gather.8.cloned.1.call-update
  86.7 0.8 constant_dynamic-slice_fusion
  87.5 4.2 reduce-scatter.3.cloned.1.call-done
  91.7 1.1 fusion.25
  92.8 1.2 fusion.28
  94.3 2.2 all_gather.17
  96.5 249.5 %all-gather.6.cloned.1.call-done = bf16[2048,5632]{1,0:T(8,128)(2,1)} async-done(((bf16[128,5632]{1,0:T(8,128)(2,1)}), bf16[2048,5632]{1,0:T(8,128)(2,1)}) %all-gather.6.cloned.1.call-update) | async-done | bytes 23068688 | tf_op jit(solution)/shard_map/all_gather | solution.py:126
  346.1 10.7 %convolution_convert_fusion = bf16[128,5632]{1,0:T(8,128)(2,1)S(1)} fusion(bf16[128,2048]{1,0:T(8,128)(2,1)S(1)} %all_gather.17, bf16[2048,5632]{1,0:T(8,128)(2,1)} %all-gather.6.cloned.1.call-done), kind=kOutput, calls=%fused_computation | convolution fusion | flops 2953510912 | bytes 25034752 | tf_op jit(solution)/shard_map/dot_general | solution.py:127
  356.8 3.4 collective-permute-start
  360.2 1.5 collective-permute-start.1
  362.1 4.4 collective-permute-done.1
  366.9 2.4 fusion.3
  369.4 160.2 %all-gather.8.cloned.1.call-done = bf16[2816,2048]{1,0:T(8,128)(2,1)} async-done(((bf16[2816,128]{1,0:T(8,128)(2,1)}), bf16[2816,2048]{1,0:T(8,128)(2,1)}) %all-gather.8.cloned.1.call-update) | async-done | bytes 11534352 | tf_op jit(solution)/shard_map/all_gather | solution.py:141
  529.5 7.7 %convolution_convert_fusion.3 = bf16[128,2048]{1,0:T(8,128)(2,1)} fusion(bf16[2816,2048]{1,0:T(8,128)(2,1)} %all-gather.8.cloned.1.call-done, f32[128,5632]{1,0:T(8,128)} %fusion.3), kind=kOutput, calls=%fused_computation.13 | convolution fusion | flops 1478819840 | bytes 14942208 | tf_op jit(solution)/shard_map/dot_general | solution.py:142
  537.3 6.2 %reduce-scatter.5.cloned.1.call-done = bf16[64,2048]{1,0:T(8,128)(2,1)} async-done(((bf16[128,2048]{1,0:T(8,128)(2,1)}), bf16[64,2048]{1,0:T(8,128)(2,1)}) %reduce-scatter.5.cloned.1.call-update) | async-done | bytes 262160 | tf_op jit(solution)/shard_map/reduce_scatter | solution.py:143
  543.5 1.1 fusion.29
  544.6 1.8 fusion.34
  (46 shorter events, 1.8 us)
Async XLA Ops:
  6.5 75.9 %copy-start = (bf16[512,2048]{1,0:T(8,128)(2,1)S(1)}, bf16[512,2048]{1,0:T(8,128)(2,1)}, u32[]{:S(2)}) copy-start(bf16[512,2048]{1,0:T(8,128)(2,1)} %param.25) | copy-start | bytes 6291460
  6.5 61.8 %all-gather.4.cloned.1.call-start = ((), (), s32[]{:S(2)}) async-start(), calls=%async_computation.2 | async-start | bytes 1114112 | tf_op jit(solution)/shard_map/all_gather | solution.py:85
  9.9 81.8 %reduce-scatter.3.cloned.1.call-start = ((), (), s32[]{:S(2)}) async-start(), calls=%async_computation.3 | async-start | bytes 786432 | tf_op jit(solution)/shard_map/reduce_scatter | solution.py:111
  75.7 1.9 copy-start.1
  75.7 2.5 copy-start.2
  82.5 2.4 copy-start.3
  82.5 2.4 copy-start.4
  84.7 2.0 copy-start.5
  84.8 2.0 copy-start.6
  84.8 261.3 %all-gather.6.cloned.1.call-start = ((), (), s32[]{:S(2)}) async-start(), calls=%async_computation.4 | async-start | bytes 24510464 | tf_op jit(solution)/shard_map/all_gather | solution.py:126
  86.1 443.5 %all-gather.8.cloned.1.call-start = ((), (), s32[]{:S(2)}) async-start(), calls=%async_computation.5 | async-start | bytes 12255232 | tf_op jit(solution)/shard_map/all_gather | solution.py:141
  86.7 456.9 %reduce-scatter.5.cloned.1.call-start = ((), (), s32[]{:S(2)}) async-start(), calls=%async_computation.6 | async-start | bytes 786432 | tf_op jit(solution)/shard_map/reduce_scatter | solution.py:143
  356.8 5.3 collective-permute-start
  360.2 6.3 %collective-permute-start.1 = (bf16[1,5632]{1,0:T(2,128)(2,1)S(1)}, bf16[1,5632]{1,0:T(2,128)(2,1)S(1)}, u32[]{:S(2)}, u32[]{:S(2)}) collective-permute-start(bf16[1,5632]{1,0:T(2,128)(2,1)S(1)} %get-tuple-element.9), channel_id=1, source_target_pairs={{2,0},{4,2},{6,4},{8,6},{10,8},{12,10},{14,12},{16,14},{18,16},{20... | collective-permute-start | bytes 33800 | tf_op jit(solution)/shard_map/ppermute | solution.py:19
  369.4 167.9 %copy-start.7 = (bf16[2048]{0:T(1024)(128)(2,1)S(1)}, bf16[2048]{0:T(1024)(128)(2,1)}, u32[]{:S(2)}) copy-start(bf16[2048]{0:T(1024)(128)(2,1)} %param.28) | copy-start | bytes 12292
Sparse Core Ops, SparseCore 0:
  10.1 58.1 all-gather.3
  84.9 6.7 reduce-scatter.2
  94.4 251.6 all-gather.5
  348.6 180.8 all-gather.7
  537.4 6.0 reduce-scatter.4
where the time goes:
time: 554 us; the launch traced here: 553 us
  waiting for transfers between devices  436 us (79%)
  blocking collectives  46.3 us (8%)
  matrix products  32.3 us (6%)
  other arithmetic  15.6 us (3%)
  between operations  13.4 us (2%)
    all_gather x1, waiting for transfers between devices, body(): up_whole = lax.all_gather(up_joined, 'sp', axis=0, tiled=True)  250 us
    all_gather x1, waiting for transfers between devices, body(): down_whole = lax.all_gather(down_weight, 'sp', axis=1, tiled=True)  160 us
    all_gather x1, blocking collectives, body(): lax.all_gather(key_turn, 'sp', axis=0, tiled=True)  44.1 us
  transfers between devices with their start and end apart: 7, of which 7 were waited for; matrix products, arithmetic and copies ran while one was open for 4% of the time, Pallas kernels for 0%

commit v1 on v0

--- a/solution.py
+++ b/solution.py
@@ -123,7 +123,12 @@
     )
     ff_dev = up_value.shape[1]
     up_joined = jnp.concatenate([up_value, up_gate], axis=1)
-    up_whole = lax.all_gather(up_joined, "sp", axis=0, tiled=True)
+    ring = [up_joined]
+    for hop in range(15):
+        ring.append(lax.ppermute(ring[-1], "sp", [(dev, (dev + 1) % 16) for dev in range(16)]))
+    up_whole = jnp.roll(
+        jnp.concatenate(ring[::-1], axis=0), (lax.axis_index("sp") + 1) * ring[0].shape[0], axis=0
+    )
     up_pair = jnp.dot(inputs, up_whole, preferred_element_type=jnp.float32).astype(jnp.bfloat16)
     padded = extended(up_pair, (("sp", 0),), 1).astype(jnp.float32)
     channel_start = tp_index * ff_dev

time: 554 us -> 748 us (1.35)
  waiting for transfers between devices: 436 us -> 547 us
  local copies, waits for them, and re-layouts: 4.22 us -> 65.7 us
  blocking collectives: 46.3 us -> 58.6 us
    ppermute x0 -> x15, waiting for transfers between devices: none -> 446 us  [body(): lax.ppermute(ring[-1], 'sp', [(dev, (dev + 1) % 16) for dev in range(16)])]
    all_gather x1 -> x0, waiting for transfers between devices: 250 us -> none  [body(): up_whole = lax.all_gather(up_joined, 'sp', axis=0, tiled=True)]
    all_gather x1, waiting for transfers between devices: 160 us -> 90 us  [body(): down_whole = lax.all_gather(down_weight, 'sp', axis=1, tiled=True)]
    unnamed x16 -> x89, local copies, waits for them, and re-layouts: 1.93 us -> 61.6 us
    all_gather x1, blocking collectives: 44.1 us -> 56.2 us  [body(): lax.all_gather(key_turn, 'sp', axis=0, tiled=True)]
    all_gather x1, waiting for transfers between devices: 10.8 us -> 0.19 us  [body(): lax.all_gather(normed, 'sp', axis=0, tiled=True)]
    ppermute x0 -> x15, starting transfers between devices: none -> 7.64 us  [body(): lax.ppermute(ring[-1], 'sp', [(dev, (dev + 1) % 16) for dev in range(16)])]
  transfers between devices with their start and end apart: 7 -> 21, of which waited for: 7 -> 19; matrix products, arithmetic and copies ran while one was open for 4% -> 13% of each run, Pallas kernels for 0% -> 0%
where the time goes in v1:
time: 748 us; the launch traced here: 747 us
  waiting for transfers between devices  547 us (73%)
  local copies, waits for them, and re-layouts  65.7 us (9%)
  blocking collectives  58.6 us (8%)
  matrix products  33 us (4%)
  other arithmetic  19.3 us (3%)
  between operations  13.5 us (2%)
  starting transfers between devices  10.4 us (1%)
    ppermute x15, waiting for transfers between devices, body(): lax.ppermute(ring[-1], 'sp', [(dev, (dev + 1) % 16) for dev in range(16)])  446 us
    all_gather x1, waiting for transfers between devices, body(): down_whole = lax.all_gather(down_weight, 'sp', axis=1, tiled=True)  90 us
    unnamed x89, local copies, waits for them, and re-layouts  61.6 us
    all_gather x1, blocking collectives, body(): lax.all_gather(key_turn, 'sp', axis=0, tiled=True)  56.2 us
  transfers between devices with their start and end apart: 21, of which 19 were waited for; matrix products, arithmetic and copies ran while one was open for 13% of the time, Pallas kernels for 0%

profile of v1, /device:TPU:0, one launch (start us, length us, event | category | flops | bytes accessed | tf_op | source)
XLA Modules:
  0.0 747.0 jit_solution(4209762442526547862)
XLA Ops:
  8.1 3.0 collective-permute-start
  11.1 35.6 %collective-permute-done = bf16[128,5632]{1,0:T(8,128)(2,1)S(1)} collective-permute-done((bf16[128,5632]{1,0:T(8,128)(2,1)S(1)}, bf16[128,5632]{1,0:T(8,128)(2,1)S(1)}, u32[]{:S(2)}, u32[]{:S(2)}) %collective-permute-start) | collective-permute-done | bytes 1441824 | tf_op jit(solution)/shard_map/ppermute | solution.py:128
  46.7 36.3 %collective-permute-done.1 = bf16[128,5632]{1,0:T(8,128)(2,1)S(1)} collective-permute-done((bf16[128,5632]{1,0:T(8,128)(2,1)S(1)}, bf16[128,5632]{1,0:T(8,128)(2,1)S(1)}, u32[]{:S(2)}, u32[]{:S(2)}) %collective-permute-start.1) | collective-permute-done | bytes 1441824 | tf_op jit(solution)/shard_map/ppermute | solution.py:128
  84.2 35.5 %collective-permute-done.2 = bf16[128,5632]{1,0:T(8,128)(2,1)S(1)} collective-permute-done((bf16[128,5632]{1,0:T(8,128)(2,1)S(1)}, bf16[128,5632]{1,0:T(8,128)(2,1)S(1)}, u32[]{:S(2)}, u32[]{:S(2)}) %collective-permute-start.2) | collective-permute-done | bytes 1441824 | tf_op jit(solution)/shard_map/ppermute | solution.py:128
  120.8 34.6 %collective-permute-done.3 = bf16[128,5632]{1,0:T(8,128)(2,1)S(1)} collective-permute-done((bf16[128,5632]{1,0:T(8,128)(2,1)S(1)}, bf16[128,5632]{1,0:T(8,128)(2,1)S(1)}, u32[]{:S(2)}, u32[]{:S(2)}) %collective-permute-start.3) | collective-permute-done | bytes 1441824 | tf_op jit(solution)/shard_map/ppermute | solution.py:128
  156.5 33.8 %collective-permute-done.4 = bf16[128,5632]{1,0:T(8,128)(2,1)S(1)} collective-permute-done((bf16[128,5632]{1,0:T(8,128)(2,1)S(1)}, bf16[128,5632]{1,0:T(8,128)(2,1)S(1)}, u32[]{:S(2)}, u32[]{:S(2)}) %collective-permute-start.4) | collective-permute-done | bytes 1441824 | tf_op jit(solution)/shard_map/ppermute | solution.py:128
  191.5 32.9 %collective-permute-done.5 = bf16[128,5632]{1,0:T(8,128)(2,1)S(1)} collective-permute-done((bf16[128,5632]{1,0:T(8,128)(2,1)S(1)}, bf16[128,5632]{1,0:T(8,128)(2,1)S(1)}, u32[]{:S(2)}, u32[]{:S(2)}) %collective-permute-start.5) | collective-permute-done | bytes 1441824 | tf_op jit(solution)/shard_map/ppermute | solution.py:128
  225.5 32.1 %collective-permute-done.6 = bf16[128,5632]{1,0:T(8,128)(2,1)S(1)} collective-permute-done((bf16[128,5632]{1,0:T(8,128)(2,1)S(1)}, bf16[128,5632]{1,0:T(8,128)(2,1)S(1)}, u32[]{:S(2)}, u32[]{:S(2)}) %collective-permute-start.6) | collective-permute-done | bytes 1441824 | tf_op jit(solution)/shard_map/ppermute | solution.py:128
  258.7 31.2 %collective-permute-done.7 = bf16[128,5632]{1,0:T(8,128)(2,1)S(1)} collective-permute-done((bf16[128,5632]{1,0:T(8,128)(2,1)S(1)}, bf16[128,5632]{1,0:T(8,128)(2,1)S(1)}, u32[]{:S(2)}, u32[]{:S(2)}) %collective-permute-start.7) | collective-permute-done | bytes 1441824 | tf_op jit(solution)/shard_map/ppermute | solution.py:128
  291.0 30.6 %collective-permute-done.8 = bf16[128,5632]{1,0:T(8,128)(2,1)S(1)} collective-permute-done((bf16[128,5632]{1,0:T(8,128)(2,1)S(1)}, bf16[128,5632]{1,0:T(8,128)(2,1)S(1)}, u32[]{:S(2)}, u32[]{:S(2)}) %collective-permute-start.8) | collective-permute-done | bytes 1441824 | tf_op jit(solution)/shard_map/ppermute | solution.py:128
  322.7 31.5 %collective-permute-done.9 = bf16[128,5632]{1,0:T(8,128)(2,1)} collective-permute-done((bf16[128,5632]{1,0:T(8,128)(2,1)S(1)}, bf16[128,5632]{1,0:T(8,128)(2,1)}, u32[]{:S(2)}, u32[]{:S(2)}) %collective-permute-start.9) | collective-permute-done | bytes 1441824 | tf_op jit(solution)/shard_map/ppermute | solution.py:128
  360.4 28.2 %collective-permute-done.10 = bf16[128,5632]{1,0:T(8,128)(2,1)} collective-permute-done((bf16[128,5632]{1,0:T(8,128)(2,1)}, bf16[128,5632]{1,0:T(8,128)(2,1)}, u32[]{:S(2)}, u32[]{:S(2)}) %collective-permute-start.10) | collective-permute-done | bytes 1441824 | tf_op jit(solution)/shard_map/ppermute | solution.py:128
  391.2 56.2 %all_gather.13 = bf16[2048,64]{0,1:T(8,128)(2,1)} all-gather(bf16[128,64]{0,1:T(8,128)(2,1)S(1)} %bitcast.40), channel_id=1, replica_groups=mesh['sp'=16,'tp'=2] {'sp'}, dimensions={0}, use_global_device_ids=true | all-gather | bytes 278528 | tf_op jit(solution)/shard_map/all_gather | solution.py:86
  449.9 4.5 fusion.13
  456.6 3.1 fusion.64
  462.2 4.7 fusion.21
  469.2 20.8 %collective-permute-done.12 = bf16[128,5632]{1,0:T(8,128)(2,1)} collective-permute-done((bf16[128,5632]{1,0:T(8,128)(2,1)}, bf16[128,5632]{1,0:T(8,128)(2,1)}, u32[]{:S(2)}, u32[]{:S(2)}) %collective-permute-start.12) | collective-permute-done | bytes 1441824 | tf_op jit(solution)/shard_map/ppermute | solution.py:128
  492.1 35.2 %collective-permute-done.13 = bf16[128,5632]{1,0:T(8,128)(2,1)S(1)} collective-permute-done((bf16[128,5632]{1,0:T(8,128)(2,1)}, bf16[128,5632]{1,0:T(8,128)(2,1)S(1)}, u32[]{:S(2)}, u32[]{:S(2)}) %collective-permute-start.13) | collective-permute-done | bytes 1441824 | tf_op jit(solution)/shard_map/ppermute | solution.py:128
  533.6 27.1 %collective-permute-done.14 = bf16[128,5632]{1,0:T(8,128)(2,1)S(1)} collective-permute-done((bf16[128,5632]{1,0:T(8,128)(2,1)S(1)}, bf16[128,5632]{1,0:T(8,128)(2,1)S(1)}, u32[]{:S(2)}, u32[]{:S(2)}) %collective-permute-start.14) | collective-permute-done | bytes 1441824 | tf_op jit(solution)/shard_map/ppermute | solution.py:128
  563.1 2.6 constant_dynamic-update-slice_fusion.29
  565.7 2.7 constant_dynamic-update-slice_fusion.28
  568.4 2.7 constant_dynamic-update-slice_fusion.27
  571.2 2.8 constant_dynamic-update-slice_fusion.26
  589.3 2.6 constant_dynamic-update-slice_fusion.13
  591.9 2.6 constant_dynamic-update-slice_fusion.12
  594.5 2.6 constant_dynamic-update-slice_fusion.11
  597.1 2.6 constant_dynamic-update-slice_fusion.10
  612.4 10.7 %fusion.2 = bf16[128,5632]{1,0:T(8,128)(2,1)S(1)} fusion(bf16[128,2048]{1,0:T(8,128)(2,1)S(1)} %all_gather.14, bf16[4096,5632]{1,0:T(8,128)(2,1)} %constant_dynamic-update-slice_fusion.32, s32[]{:T(128)S(6)} %select_n.57), kind=kOutput, calls=%fused_computation.2 | convolution fusion | flops 2953510912 | bytes 25034756 | tf_op jit(solution)/shard_map/dot_general | solution.py:132
  626.2 4.6 collective-permute-done.16
  633.6 90.0 %all-gather.5.cloned.1.call-done = bf16[2816,2048]{1,0:T(8,128)(2,1)} async-done(((bf16[2816,128]{1,0:T(8,128)(2,1)}), bf16[2816,2048]{1,0:T(8,128)(2,1)}) %all-gather.5.cloned.1.call-update) | async-done | bytes 11534352 | tf_op jit(solution)/shard_map/all_gather | solution.py:146
  723.6 7.8 %convolution_convert_fusion.2 = bf16[128,2048]{1,0:T(8,128)(2,1)} fusion(bf16[2816,2048]{1,0:T(8,128)(2,1)} %all-gather.5.cloned.1.call-done, f32[128,5632]{1,0:T(8,128)} %fusion.8), kind=kOutput, calls=%fused_computation.15 | convolution fusion | flops 1478819840 | bytes 14942208 | tf_op jit(solution)/shard_map/dot_general | solution.py:147
  731.5 6.0 reduce-scatter.5.cloned.1.call-done
  (147 shorter events, 76.2 us)
Async XLA Ops:
  6.5 460.4 %copy-start = (bf16[512,2048]{1,0:T(8,128)(2,1)S(1)}, bf16[512,2048]{1,0:T(8,128)(2,1)}, u32[]{:S(2)}) copy-start(bf16[512,2048]{1,0:T(8,128)(2,1)} %param.25) | copy-start | bytes 6291460
  6.5 443.3 %all-gather.3.cloned.1.call-start = ((), (), s32[]{:S(2)}) async-start(), calls=%async_computation.2 | async-start | bytes 1114112 | tf_op jit(solution)/shard_map/all_gather | solution.py:85
  8.1 38.6 %collective-permute-start = (bf16[128,5632]{1,0:T(8,128)(2,1)S(1)}, bf16[128,5632]{1,0:T(8,128)(2,1)S(1)}, u32[]{:S(2)}, u32[]{:S(2)}) collective-permute-start(bf16[128,5632]{1,0:T(8,128)(2,1)S(1)} %pad_maximum_fusion), channel_id=1, source_target_pairs={{0,2},{2,4},{4,6},{6,8},{8,10},{10,12},{12,14},{14,16},{16,18},{18... | collective-permute-start | bytes 4325384 | tf_op jit(solution)/shard_map/ppermute | solution.py:128
  46.7 36.3 %collective-permute-start.1 = (bf16[128,5632]{1,0:T(8,128)(2,1)S(1)}, bf16[128,5632]{1,0:T(8,128)(2,1)S(1)}, u32[]{:S(2)}, u32[]{:S(2)}) collective-permute-start(bf16[128,5632]{1,0:T(8,128)(2,1)S(1)} %collective-permute-done), channel_id=1, source_target_pairs={{0,2},{2,4},{4,6},{6,8},{8,10},{10,12},{12,14},{14,16},{16,18},{18... | collective-permute-start | bytes 4325384 | tf_op jit(solution)/shard_map/ppermute | solution.py:128
  84.2 35.5 %collective-permute-start.2 = (bf16[128,5632]{1,0:T(8,128)(2,1)S(1)}, bf16[128,5632]{1,0:T(8,128)(2,1)S(1)}, u32[]{:S(2)}, u32[]{:S(2)}) collective-permute-start(bf16[128,5632]{1,0:T(8,128)(2,1)S(1)} %collective-permute-done.1), channel_id=1, source_target_pairs={{0,2},{2,4},{4,6},{6,8},{8,10},{10,12},{12,14},{14,16},{16,18},{18... | collective-permute-start | bytes 4325384 | tf_op jit(solution)/shard_map/ppermute | solution.py:128
  120.8 34.6 %collective-permute-start.3 = (bf16[128,5632]{1,0:T(8,128)(2,1)S(1)}, bf16[128,5632]{1,0:T(8,128)(2,1)S(1)}, u32[]{:S(2)}, u32[]{:S(2)}) collective-permute-start(bf16[128,5632]{1,0:T(8,128)(2,1)S(1)} %collective-permute-done.2), channel_id=1, source_target_pairs={{0,2},{2,4},{4,6},{6,8},{8,10},{10,12},{12,14},{14,16},{16,18},{18... | collective-permute-start | bytes 4325384 | tf_op jit(solution)/shard_map/ppermute | solution.py:128
  156.5 33.8 %collective-permute-start.4 = (bf16[128,5632]{1,0:T(8,128)(2,1)S(1)}, bf16[128,5632]{1,0:T(8,128)(2,1)S(1)}, u32[]{:S(2)}, u32[]{:S(2)}) collective-permute-start(bf16[128,5632]{1,0:T(8,128)(2,1)S(1)} %collective-permute-done.3), channel_id=1, source_target_pairs={{0,2},{2,4},{4,6},{6,8},{8,10},{10,12},{12,14},{14,16},{16,18},{18... | collective-permute-start | bytes 4325384 | tf_op jit(solution)/shard_map/ppermute | solution.py:128
  191.5 32.9 %collective-permute-start.5 = (bf16[128,5632]{1,0:T(8,128)(2,1)S(1)}, bf16[128,5632]{1,0:T(8,128)(2,1)S(1)}, u32[]{:S(2)}, u32[]{:S(2)}) collective-permute-start(bf16[128,5632]{1,0:T(8,128)(2,1)S(1)} %collective-permute-done.4), channel_id=1, source_target_pairs={{0,2},{2,4},{4,6},{6,8},{8,10},{10,12},{12,14},{14,16},{16,18},{18... | collective-permute-start | bytes 4325384 | tf_op jit(solution)/shard_map/ppermute | solution.py:128
  225.5 32.1 %collective-permute-start.6 = (bf16[128,5632]{1,0:T(8,128)(2,1)S(1)}, bf16[128,5632]{1,0:T(8,128)(2,1)S(1)}, u32[]{:S(2)}, u32[]{:S(2)}) collective-permute-start(bf16[128,5632]{1,0:T(8,128)(2,1)S(1)} %collective-permute-done.5), channel_id=1, source_target_pairs={{0,2},{2,4},{4,6},{6,8},{8,10},{10,12},{12,14},{14,16},{16,18},{18... | collective-permute-start | bytes 4325384 | tf_op jit(solution)/shard_map/ppermute | solution.py:128
  258.7 31.2 %collective-permute-start.7 = (bf16[128,5632]{1,0:T(8,128)(2,1)S(1)}, bf16[128,5632]{1,0:T(8,128)(2,1)S(1)}, u32[]{:S(2)}, u32[]{:S(2)}) collective-permute-start(bf16[128,5632]{1,0:T(8,128)(2,1)S(1)} %collective-permute-done.6), channel_id=1, source_target_pairs={{0,2},{2,4},{4,6},{6,8},{8,10},{10,12},{12,14},{14,16},{16,18},{18... | collective-permute-start | bytes 4325384 | tf_op jit(solution)/shard_map/ppermute | solution.py:128
  291.0 30.6 %collective-permute-start.8 = (bf16[128,5632]{1,0:T(8,128)(2,1)S(1)}, bf16[128,5632]{1,0:T(8,128)(2,1)S(1)}, u32[]{:S(2)}, u32[]{:S(2)}) collective-permute-start(bf16[128,5632]{1,0:T(8,128)(2,1)S(1)} %collective-permute-done.7), channel_id=1, source_target_pairs={{0,2},{2,4},{4,6},{6,8},{8,10},{10,12},{12,14},{14,16},{16,18},{18... | collective-permute-start | bytes 4325384 | tf_op jit(solution)/shard_map/ppermute | solution.py:128
  322.7 31.5 %collective-permute-start.9 = (bf16[128,5632]{1,0:T(8,128)(2,1)S(1)}, bf16[128,5632]{1,0:T(8,128)(2,1)}, u32[]{:S(2)}, u32[]{:S(2)}) collective-permute-start(bf16[128,5632]{1,0:T(8,128)(2,1)S(1)} %collective-permute-done.8), channel_id=1, source_target_pairs={{0,2},{2,4},{4,6},{6,8},{8,10},{10,12},{12,14},{14,16},{16,18},{18... | collective-permute-start | bytes 4325384 | tf_op jit(solution)/shard_map/ppermute | solution.py:128
  354.3 34.3 %collective-permute-start.10 = (bf16[128,5632]{1,0:T(8,128)(2,1)}, bf16[128,5632]{1,0:T(8,128)(2,1)}, u32[]{:S(2)}, u32[]{:S(2)}) collective-permute-start(bf16[128,5632]{1,0:T(8,128)(2,1)} %collective-permute-done.9), channel_id=1, source_target_pairs={{0,2},{2,4},{4,6},{6,8},{8,10},{10,12},{12,14},{14,16},{16,18},{18... | collective-permute-start | bytes 4325384 | tf_op jit(solution)/shard_map/ppermute | solution.py:128
  357.5 133.5 %reduce-scatter.3.cloned.1.call-start = ((), (), s32[]{:S(2)}) async-start(), calls=%async_computation.3 | async-start | bytes 786432 | tf_op jit(solution)/shard_map/reduce_scatter | solution.py:111
  388.6 65.8 %collective-permute-start.11 = (bf16[128,5632]{1,0:T(8,128)(2,1)}, bf16[128,5632]{1,0:T(8,128)(2,1)}, u32[]{:S(2)}, u32[]{:S(2)}) collective-permute-start(bf16[128,5632]{1,0:T(8,128)(2,1)} %collective-permute-done.10), channel_id=1, source_target_pairs={{0,2},{2,4},{4,6},{6,8},{8,10},{10,12},{12,14},{14,16},{16,18},{18... | collective-permute-start | bytes 4325384 | tf_op jit(solution)/shard_map/ppermute | solution.py:128
  454.4 35.6 %collective-permute-start.12 = (bf16[128,5632]{1,0:T(8,128)(2,1)}, bf16[128,5632]{1,0:T(8,128)(2,1)}, u32[]{:S(2)}, u32[]{:S(2)}) collective-permute-start(bf16[128,5632]{1,0:T(8,128)(2,1)} %collective-permute-done.11), channel_id=1, source_target_pairs={{0,2},{2,4},{4,6},{6,8},{8,10},{10,12},{12,14},{14,16},{16,18},{18... | collective-permute-start | bytes 4325384 | tf_op jit(solution)/shard_map/ppermute | solution.py:128
  462.2 27.9 %copy-start.25 = (bf16[2048]{0:T(1024)(128)(2,1)S(1)}, bf16[2048]{0:T(1024)(128)(2,1)}, u32[]{:S(2)}) copy-start(bf16[2048]{0:T(1024)(128)(2,1)} %param.26) | copy-start | bytes 12292
  462.2 27.9 %copy-start.26 = (bf16[2048]{0:T(1024)(128)(2,1)S(1)}, bf16[2048]{0:T(1024)(128)(2,1)}, u32[]{:S(2)}) copy-start(bf16[2048]{0:T(1024)(128)(2,1)} %param.27) | copy-start | bytes 12292
  469.2 254.4 %all-gather.5.cloned.1.call-start = ((), (), s32[]{:S(2)}) async-start(), calls=%async_computation.4 | async-start | bytes 12255232 | tf_op jit(solution)/shard_map/all_gather | solution.py:146
  490.0 37.3 %collective-permute-start.13 = (bf16[128,5632]{1,0:T(8,128)(2,1)}, bf16[128,5632]{1,0:T(8,128)(2,1)S(1)}, u32[]{:S(2)}, u32[]{:S(2)}) collective-permute-start(bf16[128,5632]{1,0:T(8,128)(2,1)} %collective-permute-done.12), channel_id=1, source_target_pairs={{0,2},{2,4},{4,6},{6,8},{8,10},{10,12},{12,14},{14,16},{16,18},{18... | collective-permute-start | bytes 4325384 | tf_op jit(solution)/shard_map/ppermute | solution.py:128
  490.1 247.4 %reduce-scatter.5.cloned.1.call-start = ((), (), s32[]{:S(2)}) async-start(), calls=%async_computation.5 | async-start | bytes 786432 | tf_op jit(solution)/shard_map/reduce_scatter | solution.py:148
  527.3 38.4 %copy-start.21 = (bf16[128,5632]{1,0:T(8,128)(2,1)}, bf16[128,5632]{1,0:T(8,128)(2,1)S(1)}, u32[]{:S(2)}) copy-start(bf16[128,5632]{1,0:T(8,128)(2,1)S(1)} %collective-permute-done.13) | copy-start | bytes 4325380
  527.3 33.4 %collective-permute-start.14 = (bf16[128,5632]{1,0:T(8,128)(2,1)S(1)}, bf16[128,5632]{1,0:T(8,128)(2,1)S(1)}, u32[]{:S(2)}, u32[]{:S(2)}) collective-permute-start(bf16[128,5632]{1,0:T(8,128)(2,1)S(1)} %collective-permute-done.13), channel_id=1, source_target_pairs={{0,2},{2,4},{4,6},{6,8},{8,10},{10,12},{12,14},{14,16},{16,18},{18... | collective-permute-start | bytes 4325384 | tf_op jit(solution)/shard_map/ppermute | solution.py:128
  530.9 34.8 %copy-start.23 = (bf16[64,2048]{1,0:T(8,128)(2,1)}, bf16[64,2048]{1,0:T(8,128)(2,1)S(1)}, u32[]{:S(2)}) copy-start(bf16[64,2048]{1,0:T(8,128)(2,1)S(1)} %fusion.33) | copy-start | bytes 786436
  565.7 8.3 %copy-start.20 = (bf16[128,5632]{1,0:T(8,128)(2,1)S(1)}, bf16[128,5632]{1,0:T(8,128)(2,1)}, u32[]{:S(2)}) copy-start(bf16[128,5632]{1,0:T(8,128)(2,1)} %copy-done.19) | copy-start | bytes 4325380
  568.4 6.8 copy-start.18
  571.2 5.2 copy-start.16
  623.2 3.0 collective-permute-start.15
  624.5 6.3 collective-permute-start.16
  633.6 97.8 %copy-start.27 = (bf16[2048]{0:T(1024)(128)(2,1)S(1)}, bf16[2048]{0:T(1024)(128)(2,1)}, u32[]{:S(2)}) copy-start(bf16[2048]{0:T(1024)(128)(2,1)} %param.28) | copy-start | bytes 12292
  633.6 105.0 %copy-start.24 = (bf16[64,2048]{1,0:T(8,128)(2,1)S(1)}, bf16[64,2048]{1,0:T(8,128)(2,1)}, u32[]{:S(2)}) copy-start(bf16[64,2048]{1,0:T(8,128)(2,1)} %copy-done.23) | copy-start | bytes 786436
  723.6 16.8 %copy-start.1 = (bf16[512,2048]{1,0:T(8,128)(2,1)S(1)}, bf16[512,2048]{1,0:T(8,128)(2,1)}, u32[]{:S(2)}) copy-start(bf16[512,2048]{1,0:T(8,128)(2,1)} %param.25) | copy-start | bytes 6291460
  (17 other events, 40.5 us)
Sparse Core Ops, SparseCore 0:
  357.6 92.2 all-gather.2
  469.3 7.0 reduce-scatter.2
  490.2 233.3 all-gather.4
  731.6 5.8 reduce-scatter.4
